TPU v7x, 32 devices: a whole 2x2x4 slice. The times are simulated.
32 devices in a mesh: row: 8 (over z, x), col: 4 (over y, core).
Axes of the slice: x: 2, y: 2, z: 4, core: 2. Of those that a mesh axis runs over, the one named last changes fastest.
Arguments:
- tokens: bfloat16 [1024, 4096], P('row'), may hold values from -6 to 6
- w_value: bfloat16 [2304, 4096], P('col'), may hold values from -0.09375 to 0.09375
- w_gate_one: bfloat16 [2304, 4096], P('col'), may hold values from -0.09375 to 0.09375
- w_gate_two: bfloat16 [2304, 4096], P('col'), may hold values from -0.09375 to 0.09375
- short_taps: float32 [3, 3, 2304], P(None, None, 'col'), may hold values from -3.5 to 3.5
- filter_in: float32 [33, 64], replicated, may hold values from -1 to 1
- filter_mid: float32 [64, 64], replicated, may hold values from -0.75 to 0.75
- filter_out: float32 [64, 2, 2, 2304], replicated, may hold values from -1 to 1
- decay_rate: float32 [2304], P('col'), may hold values from 0.5 to 9, as said below
- skip: float32 [2, 2304], P(None, 'col'), may hold values from -0.3 to 0.3
- w_out: bfloat16 [2304, 4096], P(None, 'col'), may hold values from -0.125 to 0.125
Outputs:
- mixed: bfloat16 [1024, 4096], P('row', 'col')
Inputs may be any that keep to these rules, and one draw needn't show every extreme that they name: `decay_rate`: each channel's rate is positive; per unit of the relative position t.
All inputs are finite; a program needn't handle non-finite values.
Results may differ from a plain program's by a relative error of at most 0.007.
Values may be sent and summed in bfloat16 or wider, within the bound.
A program may use at most 64 MiB of HBM per device.

v0:
```python
import functools
import math

import jax
import jax.numpy as jnp
import numpy as np
from jax import lax
from jax.experimental import pallas as pl
from jax.experimental.pallas import tpu as pltpu
from jax.sharding import PartitionSpec as P

BANDS = 16


HIGHEST = lax.Precision.HIGHEST


def tables(row_count, col_count, modulus):
    product = (
        jnp.arange(row_count, dtype=jnp.int32)[:, None]
        * jnp.arange(col_count, dtype=jnp.int32)[None, :]
        % modulus
    )
    angles = product.astype(jnp.float32) * (2 * math.pi / modulus)
    return (jnp.cos(angles), jnp.sin(angles))


def forward_transform(signal, in_count, wide, block_len):
    leading = signal.shape[:-1]
    inner_b = min(block_len, 128)
    inner_a = block_len // inner_b
    shaped = signal.reshape(leading + (in_count, block_len))
    cos_one, sin_one = tables(wide, in_count, wide)
    real_part = jnp.einsum("kn,...nt->...kt", cos_one, shaped, precision=HIGHEST)
    imag_part = -jnp.einsum("kn,...nt->...kt", sin_one, shaped, precision=HIGHEST)
    cos_two, sin_two = tables(wide, block_len, wide * block_len)
    real_part, imag_part = (
        real_part * cos_two + imag_part * sin_two,
        imag_part * cos_two - real_part * sin_two,
    )
    real_part = real_part.reshape(leading + (wide, inner_a, inner_b))
    imag_part = imag_part.reshape(leading + (wide, inner_a, inner_b))
    cos_three, sin_three = tables(inner_a, inner_a, inner_a)
    real_part, imag_part = (
        jnp.einsum("ja,...kab->...kjb", cos_three, real_part, precision=HIGHEST)
        + jnp.einsum("ja,...kab->...kjb", sin_three, imag_part, precision=HIGHEST),
        jnp.einsum("ja,...kab->...kjb", cos_three, imag_part, precision=HIGHEST)
        - jnp.einsum("ja,...kab->...kjb", sin_three, real_part, precision=HIGHEST),
    )
    cos_four, sin_four = tables(inner_a, inner_b, block_len)
    real_part, imag_part = (
        real_part * cos_four + imag_part * sin_four,
        imag_part * cos_four - real_part * sin_four,
    )
    cos_five, sin_five = tables(inner_b, inner_b, inner_b)
    return (
        jnp.einsum("...jb,bm->...jm", real_part, cos_five, precision=HIGHEST)
        + jnp.einsum("...jb,bm->...jm", imag_part, sin_five, precision=HIGHEST),
        jnp.einsum("...jb,bm->...jm", imag_part, cos_five, precision=HIGHEST)
        - jnp.einsum("...jb,bm->...jm", real_part, sin_five, precision=HIGHEST),
    )


def inverse_transform(real_part, imag_part, out_count, wide, block_len):
    leading = real_part.shape[:-3]
    inner_b = min(block_len, 128)
    inner_a = block_len // inner_b
    cos_five, sin_five = tables(inner_b, inner_b, inner_b)
    real_part, imag_part = (
        jnp.einsum("...jm,mb->...jb", real_part, cos_five, precision=HIGHEST)
        - jnp.einsum("...jm,mb->...jb", imag_part, sin_five, precision=HIGHEST),
        jnp.einsum("...jm,mb->...jb", imag_part, cos_five, precision=HIGHEST)
        + jnp.einsum("...jm,mb->...jb", real_part, sin_five, precision=HIGHEST),
    )
    cos_four, sin_four = tables(inner_a, inner_b, block_len)
    real_part, imag_part = (
        real_part * cos_four - imag_part * sin_four,
        imag_part * cos_four + real_part * sin_four,
    )
    cos_three, sin_three = tables(inner_a, inner_a, inner_a)
    real_part, imag_part = (
        jnp.einsum("aj,...kjb->...kab", cos_three, real_part, precision=HIGHEST)
        - jnp.einsum("aj,...kjb->...kab", sin_three, imag_part, precision=HIGHEST),
        jnp.einsum("aj,...kjb->...kab", cos_three, imag_part, precision=HIGHEST)
        + jnp.einsum("aj,...kjb->...kab", sin_three, real_part, precision=HIGHEST),
    )
    real_part = real_part.reshape(leading + (wide, block_len))
    imag_part = imag_part.reshape(leading + (wide, block_len))
    cos_two, sin_two = tables(wide, block_len, wide * block_len)
    real_part, imag_part = (
        real_part * cos_two - imag_part * sin_two,
        imag_part * cos_two + real_part * sin_two,
    )
    cos_one, sin_one = tables(out_count, wide, wide)
    result = jnp.einsum("nk,...kt->...nt", cos_one, real_part, precision=HIGHEST) - jnp.einsum(
        "nk,...kt->...nt", sin_one, imag_part, precision=HIGHEST
    )
    return (result / (wide * block_len)).reshape(leading + (out_count * block_len,))


def short_filter(padded, filter_taps):
    return (
        padded[..., :-2] * filter_taps[:, 0, :, None]
        + padded[..., 1:-1] * filter_taps[:, 1, :, None]
        + padded[..., 2:] * filter_taps[:, 2, :, None]
    )


def filter_bank(seq_len, filter_in, filter_mid, out_block, rate_block):
    positions = jnp.arange(seq_len, dtype=jnp.float32)
    relative = positions / (seq_len - 1)
    bands = jnp.linspace(0.0001, BANDS - 1, BANDS, dtype=jnp.float32)
    angles = 2 * math.pi / seq_len * positions[:, None] * bands[None, :]
    feats = jnp.concatenate([relative[:, None], jnp.cos(angles), jnp.sin(angles)], axis=1)
    hidden = jnp.sin(jnp.dot(feats, filter_in, precision=HIGHEST))
    hidden = jnp.sin(jnp.dot(hidden, filter_mid, precision=HIGHEST))
    filter_taps = jnp.einsum("lh,hodc->odcl", hidden, out_block, precision=HIGHEST)
    decay = jnp.exp(-relative[None, :] * rate_block[:, None])
    return filter_taps * decay


def on_device(
    tokens,
    w_value,
    w_gate_one,
    w_gate_two,
    short_taps,
    filter_in,
    filter_mid,
    filter_out,
    decay_rate,
    skip,
    w_out,
):
    n_rows = lax.axis_size("row")
    row_index = lax.axis_index("row")
    col_index = lax.axis_index("col")
    local_width = w_value.shape[0]
    chan_dev = local_width // n_rows
    projected = jnp.stack(
        [
            jnp.einsum("td,cd->ct", tokens, weight, preferred_element_type=jnp.float32)
            for weight in (w_value, w_gate_one, w_gate_two)
        ]
    ).astype(jnp.bfloat16)
    block_len = projected.shape[2]
    seq_len = n_rows * block_len
    wide = 2 * n_rows
    moved = lax.all_to_all(projected, "row", split_axis=1, concat_axis=2, tiled=True)
    own_taps = lax.dynamic_slice_in_dim(short_taps, row_index * chan_dev, chan_dev, 2)
    bordered = jnp.pad(moved.astype(jnp.float32), ((0, 0), (0, 0), (1, 1)))
    channel_major = short_filter(bordered, own_taps)
    global_start = col_index * local_width + row_index * chan_dev
    own_out = lax.dynamic_slice_in_dim(filter_out, global_start, chan_dev, 3)
    own_rate = lax.dynamic_slice_in_dim(decay_rate, row_index * chan_dev, chan_dev, 0)
    own_skip = lax.dynamic_slice_in_dim(skip, row_index * chan_dev, chan_dev, 1)
    filter_taps = filter_bank(seq_len, filter_in, filter_mid, own_out, own_rate)
    forward_part = filter_taps[:, 0]
    backward_part = filter_taps[:, 1]
    kern = jnp.concatenate(
        [
            forward_part,
            jnp.zeros(forward_part[..., :1].shape, jnp.float32),
            backward_part[..., 1:][..., ::-1],
        ],
        axis=-1,
    )
    kern_real, kern_imag = forward_transform(kern, wide, wide, block_len)
    signal = channel_major[0]
    for order_index in range(2):
        sig_real, sig_imag = forward_transform(signal, n_rows, wide, block_len)
        prod_real = sig_real * kern_real[order_index] - sig_imag * kern_imag[order_index]
        prod_imag = sig_real * kern_imag[order_index] + sig_imag * kern_real[order_index]
        long_part = inverse_transform(prod_real, prod_imag, n_rows, wide, block_len)
        signal = channel_major[order_index + 1] * (
            long_part + own_skip[order_index][:, None] * signal
        )
    mixer_channels = signal.astype(jnp.bfloat16)
    position_major = lax.all_to_all(mixer_channels, "row", split_axis=1, concat_axis=0, tiled=True)
    totals = jnp.einsum(
        "ct,cd->td",
        lax.all_gather(position_major, "col", axis=0, tiled=True),
        w_out,
        preferred_element_type=jnp.float32,
    )
    return totals.astype(jnp.bfloat16)


STEP = 32


def position_features(seq_len):
    positions = np.arange(seq_len, dtype=np.float32)
    relative = positions / np.float32(seq_len - 1)
    bands = np.linspace(0.0001, BANDS - 1, BANDS, dtype=np.float32)
    angles = np.float32(2 * math.pi / seq_len) * positions[None, :] * bands[:, None]
    return np.concatenate([relative[None, :], np.cos(angles), np.sin(angles)], axis=0)


def table_seeds(seq_len):
    odd = 2 * np.arange(seq_len)[None, :] + 1
    coarse = (STEP * np.arange(seq_len // STEP)[:, None] * odd) % (4 * seq_len)
    fine = (np.arange(STEP)[:, None] * odd) % (4 * seq_len)
    unit = math.pi / (2 * seq_len)
    return (
        np.stack([np.cos(coarse * unit), np.sin(coarse * unit)]).astype(np.float32),
        np.stack([np.cos(fine * unit), np.sin(fine * unit)]).astype(np.float32),
    )


def split_dot(left, table, table_dim):
    high = left.astype(jnp.bfloat16)
    low = (left - high.astype(jnp.float32)).astype(jnp.bfloat16)
    both = jnp.concatenate([high, low], axis=0)
    product = lax.dot_general(
        both, table, (((1,), (table_dim,)), ((), ())), preferred_element_type=jnp.float32
    )
    return product[: left.shape[0]] + product[left.shape[0] :]


def exact_dot(left, right, left_dim):
    return lax.dot_general(
        left,
        right,
        (((left_dim,), (0,)), ((), ())),
        precision=HIGHEST,
        preferred_element_type=jnp.float32,
    )


def make_tables(coarse_ref, fine_ref, cos_ref, sin_ref):
    def fill(index, carry):
        cos_a = coarse_ref[0, pl.ds(index, 1), :]
        sin_a = coarse_ref[1, pl.ds(index, 1), :]
        cos_b = fine_ref[0]
        sin_b = fine_ref[1]
        rows = pl.ds(pl.multiple_of(index * STEP, STEP), STEP)
        cos_ref[rows, :] = (cos_a * cos_b - sin_a * sin_b).astype(jnp.bfloat16)
        sin_ref[rows, :] = (sin_a * cos_b + cos_a * sin_b).astype(jnp.bfloat16)
        return carry

    lax.fori_loop(0, cos_ref.shape[0] // STEP, fill, 0)


def own_column(vector, chan_dev):
    width = vector.shape[1]
    lanes = lax.broadcasted_iota(jnp.int32, (chan_dev, width), 1)
    wanted = lax.broadcasted_iota(jnp.int32, (chan_dev, width), 0) + lax.axis_index("row") * chan_dev
    return jnp.sum(jnp.where(lanes == wanted, vector, 0.0), axis=1, keepdims=True)


def kernel_spectra(chan_dev, in_ref, mid_ref, out_ref, rate_ref, feats_ref, cos_ref, sin_ref):
    hidden = jnp.sin(exact_dot(in_ref[...], feats_ref[...], 0))
    hidden = jnp.sin(exact_dot(mid_ref[...], hidden, 0))
    decay = jnp.exp(-feats_ref[0:1, :] * own_column(rate_ref[...], chan_dev))
    not_first = lax.broadcasted_iota(jnp.int32, decay.shape, 1) > 0
    sums, differences = [], []
    for order in range(2):
        ahead = exact_dot(out_ref[order, 0], hidden, 1) * decay
        behind = jnp.where(not_first, exact_dot(out_ref[order, 1], hidden, 1) * decay, 0.0)
        sums.append(ahead + behind)
        differences.append(ahead - behind)
    scale = 1.0 / cos_ref.shape[0]
    kern_cos = split_dot(jnp.concatenate(sums, axis=0), cos_ref[...], 0) * scale
    kern_sin = split_dot(jnp.concatenate(differences, axis=0), sin_ref[...], 0) * scale
    return kern_cos, kern_sin


def short_rows(blocks, short_ref, which, chan_dev):
    joined = jnp.concatenate([block.astype(jnp.float32) for block in blocks], axis=1)
    length = joined.shape[1]
    lanes = lax.broadcasted_iota(jnp.int32, joined.shape, 1)
    before = jnp.where(lanes == 0, 0.0, pltpu.roll(joined, 1, 1))
    after = jnp.where(lanes == length - 1, 0.0, pltpu.roll(joined, length - 1, 1))
    tap = [own_column(short_ref[which, j : j + 1, :], chan_dev) for j in range(3)]
    return before * tap[0] + joined * tap[1] + after * tap[2]


def long_convolutions(signals, spectra, skip_ref, cos_ref, sin_ref, chan_dev):
    kern_cos, kern_sin = spectra
    signal = signals[0]
    for order in range(2):
        rows = slice(order * chan_dev, (order + 1) * chan_dev)
        k_cos, k_sin = kern_cos[rows], kern_sin[rows]
        z_cos = split_dot(signal, cos_ref[...], 0)
        z_sin = split_dot(signal, sin_ref[...], 0)
        long_part = split_dot(z_cos * k_cos - z_sin * k_sin, cos_ref[...], 1) + split_dot(
            z_cos * k_sin + z_sin * k_cos, sin_ref[...], 1
        )
        weight = own_column(skip_ref[order : order + 1, :], chan_dev)
        signal = signals[order + 1] * (long_part + weight * signal)
    return signal


def mix_kernel(
    chan_dev,
    moved_ref,
    short_ref,
    in_ref,
    mid_ref,
    out_ref,
    rate_ref,
    skip_ref,
    feats_ref,
    coarse_ref,
    fine_ref,
    y_ref,
    cos_ref,
    sin_ref,
):
    blocks = moved_ref.shape[0]
    block_len = moved_ref.shape[3]
    make_tables(coarse_ref, fine_ref, cos_ref, sin_ref)
    spectra = kernel_spectra(chan_dev, in_ref, mid_ref, out_ref, rate_ref, feats_ref, cos_ref, sin_ref)
    signals = [
        short_rows([moved_ref[s, which] for s in range(blocks)], short_ref, which, chan_dev)
        for which in range(3)
    ]
    signal = long_convolutions(signals, spectra, skip_ref, cos_ref, sin_ref, chan_dev)
    for s in range(blocks):
        y_ref[s] = signal[:, s * block_len : (s + 1) * block_len].astype(jnp.bfloat16)


def on_device_dense(
    tokens,
    w_value,
    w_gate_one,
    w_gate_two,
    short_taps,
    filter_in,
    filter_mid,
    filter_out,
    decay_rate,
    skip,
    w_out,
):
    n_rows = lax.axis_size("row")
    row_index = lax.axis_index("row")
    col_index = lax.axis_index("col")
    local_width = w_value.shape[0]
    chan_dev = local_width // n_rows
    block_len = tokens.shape[0]
    seq_len = n_rows * block_len
    projected = [
        jnp.einsum("td,cd->ct", tokens, weight, preferred_element_type=jnp.float32)
        .astype(jnp.bfloat16)
        .reshape(n_rows, chan_dev, block_len)
        for weight in (w_value, w_gate_one, w_gate_two)
    ]
    global_start = col_index * local_width + row_index * chan_dev
    own_out = lax.dynamic_slice_in_dim(filter_out, global_start, chan_dev, 3).transpose(1, 2, 3, 0)
    coarse, fine = table_seeds(seq_len)
    moved = lax.all_to_all(jnp.stack(projected, axis=1), "row", split_axis=0, concat_axis=0, tiled=True)
    mixer_channels = pl.pallas_call(
        functools.partial(mix_kernel, chan_dev),
        out_shape=jax.ShapeDtypeStruct((n_rows, chan_dev, block_len), jnp.bfloat16),
        in_specs=[pl.BlockSpec(memory_space=pltpu.VMEM)] * 10,
        out_specs=pl.BlockSpec(memory_space=pltpu.VMEM),
        scratch_shapes=[pltpu.VMEM((seq_len, seq_len), jnp.bfloat16)] * 2,
        compiler_params=pltpu.CompilerParams(vmem_limit_bytes=40 << 20),
    )(
        moved,
        short_taps,
        filter_in,
        filter_mid,
        own_out,
        decay_rate.reshape(1, local_width),
        skip,
        position_features(seq_len),
        coarse,
        fine,
    )
    position_major = lax.all_to_all(mixer_channels, "row", split_axis=0, concat_axis=0, tiled=True)
    totals = jnp.einsum(
        "ct,cd->td",
        lax.all_gather(position_major.reshape(local_width, block_len), "col", axis=0, tiled=True),
        w_out,
        preferred_element_type=jnp.float32,
    )
    return totals.astype(jnp.bfloat16)


def solution(mesh):
    placed = (
        P("row", None),
        P("col", None),
        P("col", None),
        P("col", None),
        P(None, None, "col"),
        P(),
        P(),
        P(),
        P("col"),
        P(None, "col"),
        P(None, "col"),
    )

    def program(tokens, w_value, *rest):
        seq_len = tokens.shape[0]
        devices = mesh.shape["row"] * mesh.shape["col"]
        dense = (
            seq_len <= 2048
            and seq_len // mesh.shape["row"] % 128 == 0
            and w_value.shape[0] // devices % 8 == 0
        )
        body = on_device_dense if dense else on_device
        return jax.shard_map(
            body, mesh=mesh, in_specs=placed, out_specs=P("row", "col"), check_vma=False
        )(tokens, w_value, *rest)

    return program
```

profile of v0, /device:TPU:0, one launch (start us, length us, event | category | flops | bytes accessed | tf_op | source)
XLA Modules:
  0.0 62.9 jit_solution(2557279229676261733)
XLA Ops:
  0.0 4.2 %convolution_convert_fusion.1 = bf16[576,128]{1,0:T(8,128)(2,1)S(1)} fusion(bf16[576,4096]{1,0:T(8,128)(2,1)} %param.17, bf16[128,4096]{1,0:T(8,128)(2,1)} %param.14), kind=kOutput, calls=%fused_computation.1 | convolution fusion | flops 604053504 | bytes 5914624 | tf_op jit(solution)/shard_map/td,cd->ct/dot_general | solution.py:345
  4.2 0.3 copy-done.9
  4.5 1.4 %convolution_convert_fusion.2 = bf16[576,128]{1,0:T(8,128)(2,1)S(1)} fusion(bf16[576,4096]{1,0:T(8,128)(2,1)S(1)} %copy-done.9, bf16[128,4096]{1,0:T(8,128)(2,1)S(1)} %copy-done.10), kind=kOutput, calls=%fused_computation.2 | convolution fusion | flops 604053504 | bytes 5914624 | tf_op jit(solution)/shard_map/td,cd->ct/dot_general | solution.py:345
  5.9 0.4 slice-done
  6.3 0.3 slice-done.1
  6.6 0.0 copy-start.5
  6.6 0.0 copy-start.7
  6.6 1.4 %convolution_convert_fusion.3 = bf16[576,128]{1,0:T(8,128)(2,1)S(1)} fusion(bf16[576,4096]{1,0:T(8,128)(2,1)S(1)} %bitcast.19, bf16[128,4096]{1,0:T(8,128)(2,1)S(1)} %copy-done.10), kind=kOutput, calls=%fused_computation.3 | convolution fusion | flops 604053504 | bytes 5914624 | tf_op jit(solution)/shard_map/td,cd->ct/dot_general | solution.py:345
  8.0 0.8 %pad_maximum_fusion = bf16[8,3,72,128]{3,2,1,0:T(8,128)(2,1)} fusion(bf16[8,1,72,128]{3,2,1,0:T(8,128)(2,1)S(1)} %bitcast.15, bf16[8,1,72,128]{3,2,1,0:T(8,128)(2,1)S(1)} %bitcast.16, bf16[8,1,72,128]{3,2,1,0:T(8,128)(2,1)S(1)} %bitcast.17), kind=kLoop, calls=%fused_computation.4 | loop fusion | flops 442368 | bytes 884736 | tf_op jit(solution)/shard_map/stack | solution.py:353
  8.8 7.3 %all-to-all-start = ((bf16[8,3,72,128]{3,2,1,0:T(8,128)(2,1)}), bf16[8,3,72,128]{3,2,1,0:T(8,128)(2,1)S(1)}, u32[]{:S(2)}, u32[]{:S(2)}) async-start(bf16[8,3,72,128]{3,2,1,0:T(8,128)(2,1)} %pad_maximum_fusion), calls=%async_computation | async-start | bytes 884736 | tf_op jit(solution)/shard_map/all_to_all | solution.py:353
  16.1 0.0 copy-done
  16.1 0.9 %constant_dynamic-slice_fusion = f32[64,2,2,72]{3,2,1,0:T(2,128)} fusion(f32[64,2,2,2304]{3,2,1,0:T(2,128)S(1)} %copy-done, s32[]{:T(128)S(6)} %select_n.3), kind=kLoop, calls=%fused_computation.5 | loop fusion | bytes 147460 | tf_op jit(solution)/shard_map/dynamic_slice | solution.py:351
  17.0 1.0 %copy.16 = f32[64,2,2,72]{0,3,2,1:T(8,128)S(1)} copy(f32[64,2,2,72]{3,2,1,0:T(2,128)} %constant_dynamic-slice_fusion) | data formatting | bytes 147456
  18.0 10.8 %all-to-all-done.moved_ref = bf16[8,3,72,128]{3,2,1,0:T(8,128)(2,1)S(1)} async-done(((bf16[8,3,72,128]{3,2,1,0:T(8,128)(2,1)}), bf16[8,3,72,128]{3,2,1,0:T(8,128)(2,1)S(1)}, u32[]{:S(2)}, u32[]{:S(2)}) %all-to-all-start) | async-done | bytes 442400 | tf_op jit(solution)/shard_map/all_to_all | solution.py:353
  28.8 0.0 copy-done.4
  28.9 0.0 copy-done.5
  28.9 0.0 copy-done.7
  28.9 0.0 copy-start.3
  28.9 0.9 %copy-done.3 = f32[33,1024]{1,0:T(8,128)S(1)} copy-done((f32[33,1024]{1,0:T(8,128)S(1)}, f32[33,1024]{1,0:T(8,128)}, u32[]{:S(2)}) %copy-start.3) | copy-done | bytes 135192
  29.8 0.7 %copy-done.6 = f32[33,64]{1,0:T(8,128)S(1)} copy-done((f32[33,64]{1,0:T(8,128)S(1)}, f32[33,64]{1,0:T(8,128)}, u32[]{:S(2)}) %copy-start.6) | copy-done | bytes 8472
  30.5 10.0 %shard_map.136 = bf16[8,72,128]{2,1,0:T(8,128)(2,1)S(1)} custom-call(bf16[8,3,72,128]{3,2,1,0:T(8,128)(2,1)S(1)} %all-to-all-done.moved_ref, f32[3,3,576]{2,1,0:T(4,128)S(1)} %copy-done.5, f32[33,64]{1,0:T(8,128)S(1)} %copy-done.6, f32[64,64]{1,0:T(8,128)S(1)} %copy-done.4, f32[2,2,72,64]{3,2,1,0:T(8,128)S(1)} %bitcast.13, f32[1,576]{1,0:T(1,128)S(1)} %reshape.6.rate_ref, ...), custom_call_target="tpu_custom_call" | custom-call | tf_op jit(solution)/shard_map/pallas_call | solution.py:354
  40.6 10.9 %all_to_all.10 = bf16[8,72,128]{2,1,0:T(8,128)(2,1)S(1)} all-to-all(bf16[8,72,128]{2,1,0:T(8,128)(2,1)S(1)} %shard_map.136), channel_id=1, replica_groups=mesh['row'=8,'col'=4] {'row'}, dimensions={0} | all-to-all | bytes 294912 | tf_op jit(solution)/shard_map/all_to_all | solution.py:373
  51.5 7.6 %all_gather.3 = bf16[2304,128]{1,0:T(8,128)(2,1)S(1)} all-gather(bf16[576,128]{1,0:T(8,128)(2,1)S(1)} %bitcast.14), channel_id=1, replica_groups=mesh['row'=8,'col'=4] {'col'}, dimensions={0}, use_global_device_ids=true | all-gather | bytes 737280 | tf_op jit(solution)/shard_map/all_gather | solution.py:376
  59.0 3.9 %convolution_convert_fusion = bf16[128,1024]{1,0:T(8,128)(2,1)} fusion(bf16[2304,128]{1,0:T(8,128)(2,1)S(1)} %all_gather.3, bf16[2304,1024]{1,0:T(8,128)(2,1)} %param.24), kind=kOutput, calls=%fused_computation | convolution fusion | flops 604110848 | bytes 5570560 | tf_op jit(solution)/shard_map/ct,cd->td/dot_general | solution.py:374
  (16 shorter events, 0.0 us)
Async XLA Ops:
  0.0 16.1 %copy-start = (f32[64,2,2,2304]{3,2,1,0:T(2,128)S(1)}, f32[64,2,2,2304]{3,2,1,0:T(2,128)}, u32[]{:S(2)}) copy-start(f32[64,2,2,2304]{3,2,1,0:T(2,128)} %param.21) | copy-start | bytes 7077892
  0.0 4.2 %copy-start.10 = (bf16[128,4096]{1,0:T(8,128)(2,1)S(1)}, bf16[128,4096]{1,0:T(8,128)(2,1)}, u32[]{:S(2)}) copy-start(bf16[128,4096]{1,0:T(8,128)(2,1)} %param.14) | copy-start | bytes 3145732
  0.0 4.5 %copy-start.9 = (bf16[576,4096]{1,0:T(8,128)(2,1)S(1)}, bf16[576,4096]{1,0:T(8,128)(2,1)}, u32[]{:S(2)}) copy-start(bf16[576,4096]{1,0:T(8,128)(2,1)} %param.16) | copy-start | bytes 14155780
  0.0 6.3 %slice-start = ((s8[4718592]{0:T(1024)(128)(4,1)}), s8[4194304]{0:T(1024)(128)(4,1)S(1)}, s32[]{:S(2)}) async-start(s8[4718592]{0:T(1024)(128)(4,1)} %bitcast.18), calls=%async_computation.2 | async-start | bytes 8388608
  4.5 2.1 %slice-start.1 = ((s8[4718592]{0:T(1024)(128)(4,1)}), s8[524288]{0:T(1024)(128)(4,1)S(1)}, s32[]{:S(2)}) async-start(s8[4718592]{0:T(1024)(128)(4,1)} %bitcast.18), calls=%async_computation.3 | async-start | bytes 1048576
  6.6 11.4 %copy-start.8 = (f32[576]{0:T(1024)S(1)}, f32[576]{0:T(1024)}, u32[]{:S(2)}) copy-start(f32[576]{0:T(1024)} %param.22) | copy-start | bytes 6916
  6.6 22.3 %copy-start.1 = (f32[2,32,1024]{2,1,0:T(8,128)S(1)}, f32[2,32,1024]{2,1,0:T(8,128)}, u32[]{:S(2)}) copy-start(f32[2,32,1024]{2,1,0:T(8,128)} %constant.24.clone.coarse_ref) | copy-start | bytes 786436
  6.6 22.3 %copy-start.2 = (f32[2,32,1024]{2,1,0:T(8,128)S(1)}, f32[2,32,1024]{2,1,0:T(8,128)}, u32[]{:S(2)}) copy-start(f32[2,32,1024]{2,1,0:T(8,128)} %constant.25.clone.fine_ref) | copy-start | bytes 786436
  6.6 22.3 %copy-start.4 = (f32[64,64]{1,0:T(8,128)S(1)}, f32[64,64]{1,0:T(8,128)}, u32[]{:S(2)}) copy-start(f32[64,64]{1,0:T(8,128)} %mid_ref.1) | copy-start | bytes 49156
  6.6 22.3 %copy-start.5 = (f32[3,3,576]{2,1,0:T(4,128)S(1)}, f32[3,3,576]{2,1,0:T(4,128)}, u32[]{:S(2)}) copy-start(f32[3,3,576]{2,1,0:T(4,128)} %short_ref.1) | copy-start | bytes 62212
  6.6 22.3 %copy-start.7 = (f32[2,576]{1,0:T(2,128)S(1)}, f32[2,576]{1,0:T(2,128)}, u32[]{:S(2)}) copy-start(f32[2,576]{1,0:T(2,128)} %skip_ref.1) | copy-start | bytes 13828
  8.8 20.0 %all-to-all-start = ((bf16[8,3,72,128]{3,2,1,0:T(8,128)(2,1)}), bf16[8,3,72,128]{3,2,1,0:T(8,128)(2,1)S(1)}, u32[]{:S(2)}, u32[]{:S(2)}) async-start(bf16[8,3,72,128]{3,2,1,0:T(8,128)(2,1)} %pad_maximum_fusion), calls=%async_computation | async-start | bytes 884736 | tf_op jit(solution)/shard_map/all_to_all | solution.py:353
  28.9 0.9 %copy-start.3 = (f32[33,1024]{1,0:T(8,128)S(1)}, f32[33,1024]{1,0:T(8,128)}, u32[]{:S(2)}) copy-start(f32[33,1024]{1,0:T(8,128)} %constant.23.clone.feats_ref) | copy-start | bytes 405508
  29.8 0.7 %copy-start.6 = (f32[33,64]{1,0:T(8,128)S(1)}, f32[33,64]{1,0:T(8,128)}, u32[]{:S(2)}) copy-start(f32[33,64]{1,0:T(8,128)} %in_ref.1) | copy-start | bytes 25348
where the time goes:
time: 63.2 us; the launch traced here: 62.9 us
  blocking collectives  18.4 us (29%)
  matrix products  10.8 us (17%)
  waiting for transfers between devices  10.8 us (17%)
  Pallas kernels  10 us (16%)
  starting transfers between devices  7.28 us (12%)
  local copies, waits for them, and re-layouts  4.53 us (7%)
  other arithmetic  0.81 us (1%)
    all_to_all x1, blocking collectives, on_device_dense(): lax.all_to_all(mixer_channels, 'row', split_axis=0, concat_axis=0, tiled=...  10.9 us
    all_to_all x1, waiting for transfers between devices, on_device_dense(): lax.all_to_all(jnp.stack(projected, axis=1), 'row', split_axis=0, concat_...  10.8 us
    pallas_call x1, Pallas kernels, on_device_dense(): pl.pallas_call(functools.partial(mix_kernel, chan_dev), out_shape=jax.Sha...  10 us
    all_gather x1, blocking collectives, on_device_dense(): lax.all_gather(position_major.reshape(local_width, block_len), 'col', axi...  7.55 us
    all_to_all x1, starting transfers between devices, on_device_dense(): lax.all_to_all(jnp.stack(projected, axis=1), 'row', split_axis=0, concat_...  7.28 us
    dot_general x3, matrix products, on_device_dense(): jnp.einsum('td,cd->ct', tokens, weight, preferred_element_type=jnp.float32)  6.95 us
    dot_general x1, matrix products, on_device_dense(): jnp.einsum('ct,cd->td', lax.all_gather(position_major.reshape(local_width...  3.85 us
    unnamed x27, local copies, waits for them, and re-layouts  3.66 us
  transfers between devices with their start and end apart: 1, of which 1 were waited for; matrix products, arithmetic and copies ran while one was open for 3% of the time, Pallas kernels for 0%

commit v1 on v0

--- a/solution.py
+++ b/solution.py
@@ -276,9 +276,9 @@
     return before * tap[0] + joined * tap[1] + after * tap[2]
 
 
-def long_convolutions(signals, spectra, skip_ref, cos_ref, sin_ref, chan_dev):
+def long_convolutions(signal_of, spectra, skip_ref, cos_ref, sin_ref, chan_dev):
     kern_cos, kern_sin = spectra
-    signal = signals[0]
+    signal = signal_of(0)
     for order in range(2):
         rows = slice(order * chan_dev, (order + 1) * chan_dev)
         k_cos, k_sin = kern_cos[rows], kern_sin[rows]
@@ -288,13 +288,17 @@
             z_cos * k_sin + z_sin * k_cos, sin_ref[...], 1
         )
         weight = own_column(skip_ref[order : order + 1, :], chan_dev)
-        signal = signals[order + 1] * (long_part + weight * signal)
+        signal = signal_of(order + 1) * (long_part + weight * signal)
     return signal
 
 
 def mix_kernel(
+    n_rows,
+    n_cols,
     chan_dev,
-    moved_ref,
+    value_ref,
+    first_ref,
+    second_ref,
     short_ref,
     in_ref,
     mid_ref,
@@ -304,21 +308,117 @@
     feats_ref,
     coarse_ref,
     fine_ref,
-    y_ref,
+    gathered_ref,
     cos_ref,
     sin_ref,
+    moved_ref,
+    y_ref,
+    there_send,
+    there_recv,
+    back_send,
+    back_recv,
+    far_send,
+    far_recv,
+    mate_send,
+    mate_recv,
 ):
-    blocks = moved_ref.shape[0]
+    row = lax.axis_index("row")
+    col = lax.axis_index("col")
     block_len = moved_ref.shape[3]
+    half = n_cols // 2
+    mate = col + 1 - 2 * (col % 2)
+    projected = (value_ref, first_ref, second_ref)
+
+    def copy(source, target, send_sem, recv_sem, to_row, to_col):
+        return pltpu.make_async_remote_copy(
+            src_ref=source,
+            dst_ref=target,
+            send_sem=send_sem,
+            recv_sem=recv_sem,
+            device_id=(to_row, to_col),
+            device_id_type=pl.DeviceIdType.MESH,
+        )
+
+    def row_at(offset):
+        return (row + offset) % n_rows
+
+    def far_at(offset):
+        return (col + 2 * offset) % n_cols
+
+    partners = [(row_at(d), col) for d in range(1, n_rows)]
+    partners += [(row, far_at(h)) for h in range(1, half)] + [(row, mate)]
+    barrier = pltpu.get_barrier_semaphore()
+    for partner in partners:
+        pl.semaphore_signal(barrier, inc=1, device_id=partner, device_id_type=pl.DeviceIdType.MESH)
+    pl.semaphore_wait(barrier, len(partners))
+
+    there = {}
+    for which in range(3):
+        for d in range(1, n_rows):
+            there[which, d] = copy(
+                projected[which].at[row_at(d)],
+                moved_ref.at[which, row],
+                there_send.at[which, d - 1],
+                there_recv.at[which, d - 1],
+                row_at(d),
+                col,
+            )
+            there[which, d].start()
+    for which in range(3):
+        moved_ref[which, row] = projected[which][row]
+
     make_tables(coarse_ref, fine_ref, cos_ref, sin_ref)
     spectra = kernel_spectra(chan_dev, in_ref, mid_ref, out_ref, rate_ref, feats_ref, cos_ref, sin_ref)
-    signals = [
-        short_rows([moved_ref[s, which] for s in range(blocks)], short_ref, which, chan_dev)
-        for which in range(3)
-    ]
-    signal = long_convolutions(signals, spectra, skip_ref, cos_ref, sin_ref, chan_dev)
-    for s in range(blocks):
+
+    def signal_of(which):
+        for d in range(1, n_rows):
+            there[which, d].wait_recv()
+        return short_rows(
+            [moved_ref[which, s] for s in range(n_rows)], short_ref, which, chan_dev
+        )
+
+    signal = long_convolutions(signal_of, spectra, skip_ref, cos_ref, sin_ref, chan_dev)
+    for s in range(n_rows):
         y_ref[s] = signal[:, s * block_len : (s + 1) * block_len].astype(jnp.bfloat16)
+    gathered_ref[col, row] = y_ref[row]
+
+    back = {}
+    for d in range(1, n_rows):
+        back[d] = copy(
+            y_ref.at[row_at(d)],
+            gathered_ref.at[col, row],
+            back_send.at[d - 1],
+            back_recv.at[d - 1],
+            row_at(d),
+            col,
+        )
+        back[d].start()
+    far, near = {}, {}
+
+    def to_mate(h, d):
+        block = gathered_ref.at[far_at(h), row_at(n_rows - d)]
+        near[h, d] = copy(block, block, mate_send.at[h, d], mate_recv.at[h, d], row, mate)
+        near[h, d].start()
+
+    for d in range(n_rows):
+        if d:
+            back[d].wait_recv()
+        block = gathered_ref.at[col, row_at(n_rows - d)]
+        for h in range(1, half):
+            far[h, d] = copy(
+                block, block, far_send.at[h - 1, d], far_recv.at[h - 1, d], row, far_at(h)
+            )
+            far[h, d].start()
+        to_mate(0, d)
+    for h in range(1, half):
+        for d in range(n_rows):
+            far[h, d].wait_recv()
+            to_mate(half - h, d)
+    for send in (there, back, far, near):
+        for one in send.values():
+            one.wait_send()
+    for one in near.values():
+        one.wait_recv()
 
 
 def on_device_dense(
@@ -350,16 +450,33 @@
     global_start = col_index * local_width + row_index * chan_dev
     own_out = lax.dynamic_slice_in_dim(filter_out, global_start, chan_dev, 3).transpose(1, 2, 3, 0)
     coarse, fine = table_seeds(seq_len)
-    moved = lax.all_to_all(jnp.stack(projected, axis=1), "row", split_axis=0, concat_axis=0, tiled=True)
-    mixer_channels = pl.pallas_call(
-        functools.partial(mix_kernel, chan_dev),
-        out_shape=jax.ShapeDtypeStruct((n_rows, chan_dev, block_len), jnp.bfloat16),
-        in_specs=[pl.BlockSpec(memory_space=pltpu.VMEM)] * 10,
+    n_cols = lax.axis_size("col")
+    half = n_cols // 2
+    dma = pltpu.SemaphoreType.DMA
+    gathered = pl.pallas_call(
+        functools.partial(mix_kernel, n_rows, n_cols, chan_dev),
+        out_shape=jax.ShapeDtypeStruct((n_cols, n_rows, chan_dev, block_len), jnp.bfloat16),
+        in_specs=[pl.BlockSpec(memory_space=pltpu.VMEM)] * 12,
         out_specs=pl.BlockSpec(memory_space=pltpu.VMEM),
-        scratch_shapes=[pltpu.VMEM((seq_len, seq_len), jnp.bfloat16)] * 2,
-        compiler_params=pltpu.CompilerParams(vmem_limit_bytes=40 << 20),
+        scratch_shapes=[
+            pltpu.VMEM((seq_len, seq_len), jnp.bfloat16),
+            pltpu.VMEM((seq_len, seq_len), jnp.bfloat16),
+            pltpu.VMEM((3, n_rows, chan_dev, block_len), jnp.bfloat16),
+            pltpu.VMEM((n_rows, chan_dev, block_len), jnp.bfloat16),
+            dma((3, n_rows - 1)),
+            dma((3, n_rows - 1)),
+            dma((n_rows - 1,)),
+            dma((n_rows - 1,)),
+            dma((half - 1, n_rows)),
+            dma((half - 1, n_rows)),
+            dma((half, n_rows)),
+            dma((half, n_rows)),
+        ],
+        compiler_params=pltpu.CompilerParams(
+            vmem_limit_bytes=26 << 20, collective_id=0, has_side_effects=True
+        ),
     )(
-        moved,
+        *projected,
         short_taps,
         filter_in,
         filter_mid,
@@ -370,10 +487,9 @@
         coarse,
         fine,
     )
-    position_major = lax.all_to_all(mixer_channels, "row", split_axis=0, concat_axis=0, tiled=True)
     totals = jnp.einsum(
         "ct,cd->td",
-        lax.all_gather(position_major.reshape(local_width, block_len), "col", axis=0, tiled=True),
+        gathered.reshape(n_cols * local_width, block_len),
         w_out,
         preferred_element_type=jnp.float32,
     )
@@ -398,10 +514,13 @@
     def program(tokens, w_value, *rest):
         seq_len = tokens.shape[0]
         devices = mesh.shape["row"] * mesh.shape["col"]
+        columns = mesh.shape["col"]
         dense = (
             seq_len <= 2048
             and seq_len // mesh.shape["row"] % 128 == 0
             and w_value.shape[0] // devices % 8 == 0
+            and columns % 2 == 0
+            and columns > 2
         )
         body = on_device_dense if dense else on_device
         return jax.shard_map(

time: 63.2 us -> 40.9 us (0.65)
  Pallas kernels: 10 us -> 29.8 us
  blocking collectives: 18.4 us -> 0 us
  waiting for transfers between devices: 10.8 us -> 0 us
  starting transfers between devices: 7.28 us -> 0 us
  local copies, waits for them, and re-layouts: 4.53 us -> 2.19 us
  matrix products: 10.8 us -> 8.56 us
  other arithmetic: 0.81 us -> 0.01 us
    pallas_call x1, Pallas kernels: 10 us -> 29.8 us  [on_device_dense(): pl.pallas_call(functools.partial(mix_kernel, n_rows, n_cols, chan_dev), o...]
    all_to_all x1 -> x0, blocking collectives: 10.9 us -> none  [on_device_dense(): lax.all_to_all(mixer_channels, 'row', split_axis=0, concat_axis=0, tiled=...]
    all_to_all x1 -> x0, waiting for transfers between devices: 10.8 us -> none  [on_device_dense(): lax.all_to_all(jnp.stack(projected, axis=1), 'row', split_axis=0, concat_...]
    all_gather x1 -> x0, blocking collectives: 7.55 us -> none  [on_device_dense(): lax.all_gather(position_major.reshape(local_width, block_len), 'col', axi...]
    all_to_all x1 -> x0, starting transfers between devices: 7.28 us -> none  [on_device_dense(): lax.all_to_all(jnp.stack(projected, axis=1), 'row', split_axis=0, concat_...]
    unnamed x27 -> x29, local copies, waits for them, and re-layouts: 3.66 us -> 1.15 us
    dot_general x1, matrix products: 3.85 us -> 1.54 us  [on_device_dense(): jnp.einsum('ct,cd->td', gathered.reshape(n_cols * local_width, block_len)...]
    reshape x1, local copies, waits for them, and re-layouts: 0.01 us -> 0.84 us  [on_device_dense(): decay_rate.reshape(1, local_width)]
  transfers between devices with their start and end apart: 1 -> 0, of which waited for: 1 -> 0; matrix products, arithmetic and copies ran while one was open for 3% -> 0% of each run, Pallas kernels for 0% -> 0%
where the time goes in v1:
time: 40.9 us; the launch traced here: 40.8 us
  Pallas kernels  29.8 us (73%)
  matrix products  8.56 us (21%)
  local copies, waits for them, and re-layouts  2.19 us (5%)
    pallas_call x1, Pallas kernels, on_device_dense(): pl.pallas_call(functools.partial(mix_kernel, n_rows, n_cols, chan_dev), o...  29.8 us
    dot_general x3, matrix products, on_device_dense(): jnp.einsum('td,cd->ct', tokens, weight, preferred_element_type=jnp.float32)  7.03 us
    dot_general x1, matrix products, on_device_dense(): jnp.einsum('ct,cd->td', gathered.reshape(n_cols * local_width, block_len)...  1.54 us
    unnamed x29, local copies, waits for them, and re-layouts  1.15 us
    reshape x1, local copies, waits for them, and re-layouts, on_device_dense(): decay_rate.reshape(1, local_width)  0.84 us

profile of v1, /device:TPU:0, one launch (start us, length us, event | category | flops | bytes accessed | tf_op | source)
XLA Modules:
  0.0 40.8 jit_solution(6603882170847260741)
XLA Ops:
  0.0 0.8 %reshape.18.rate_ref = f32[1,576]{1,0:T(1,128)S(1)} reshape(f32[576]{0:T(1024)} %param.22) | data formatting | bytes 4608 | tf_op jit(solution)/shard_map/reshape | solution.py:484
  0.8 0.8 %copy-done = f32[64,2,2,2304]{3,2,1,0:T(2,128)S(1)} copy-done((f32[64,2,2,2304]{3,2,1,0:T(2,128)S(1)}, f32[64,2,2,2304]{3,2,1,0:T(2,128)}, u32[]{:S(2)}) %copy-start) | copy-done | bytes 2359320
  1.7 0.2 constant_dynamic-slice_fusion
  1.9 0.1 copy.16
  2.0 0.0 copy-start.8
  2.0 0.0 copy-start.9
  2.0 0.0 slice-start.2
  2.0 4.2 %convolution_convert_fusion.3 = bf16[576,128]{1,0:T(8,128)(2,1)S(1)} fusion(bf16[576,4096]{1,0:T(8,128)(2,1)} %param.15, bf16[128,4096]{1,0:T(8,128)(2,1)} %param.14), kind=kOutput, calls=%fused_computation.3 | convolution fusion | flops 604053504 | bytes 5914624 | tf_op jit(solution)/shard_map/td,cd->ct/dot_general | solution.py:445
  6.2 0.0 slice-start.3
  6.2 0.1 copy-done.9
  6.4 1.5 %convolution_convert_fusion.2 = bf16[576,128]{1,0:T(8,128)(2,1)S(1)} fusion(bf16[576,4096]{1,0:T(8,128)(2,1)S(1)} %copy-done.8, bf16[128,4096]{1,0:T(8,128)(2,1)S(1)} %copy-done.9), kind=kOutput, calls=%fused_computation.2 | convolution fusion | flops 604053504 | bytes 5914624 | tf_op jit(solution)/shard_map/td,cd->ct/dot_general | solution.py:445
  7.8 0.0 copy-start.1
  7.8 0.0 copy-start.2
  7.9 0.0 copy-start.3
  7.9 0.0 copy-start.4
  7.9 0.0 copy-start.5
  7.9 0.0 copy-start.6
  7.9 0.0 copy-start.7
  7.9 0.0 slice-done.2
  7.9 0.0 slice-done.3
  8.0 0.0 slice-start.1
  8.0 1.4 %convolution_convert_fusion.1 = bf16[576,128]{1,0:T(8,128)(2,1)S(1)} fusion(bf16[576,4096]{1,0:T(8,128)(2,1)S(1)} %bitcast.21, bf16[128,4096]{1,0:T(8,128)(2,1)S(1)} %copy-done.9), kind=kOutput, calls=%fused_computation.1 | convolution fusion | flops 604053504 | bytes 5914624 | tf_op jit(solution)/shard_map/td,cd->ct/dot_general | solution.py:445
  9.4 29.8 %shard_map.136 = bf16[4,8,72,128]{3,2,1,0:T(8,128)(2,1)S(1)} custom-call(bf16[8,72,128]{2,1,0:T(8,128)(2,1)S(1)} %bitcast.15, bf16[8,72,128]{2,1,0:T(8,128)(2,1)S(1)} %bitcast.16, bf16[8,72,128]{2,1,0:T(8,128)(2,1)S(1)} %bitcast.17, f32[3,3,576]{2,1,0:T(4,128)S(1)} %copy-done.5, f32[33,64]{1,0:T(8,128)S(1)} %copy-done.6, f32[64,64]{1,0:T(8,128)S(1)} %copy-done.4, ...), custom_call_target="tpu_custom_call" | custom-call | tf_op jit(solution)/shard_map/pallas_call | solution.py:456
  39.2 1.5 %convolution_convert_fusion = bf16[128,1024]{1,0:T(8,128)(2,1)} fusion(bf16[2304,128]{1,0:T(8,128)(2,1)S(1)} %bitcast.13, bf16[2304,1024]{1,0:T(8,128)(2,1)S(1)} %bitcast.19), kind=kOutput, calls=%fused_computation | convolution fusion | flops 604110848 | bytes 5570560 | tf_op jit(solution)/shard_map/ct,cd->td/dot_general | solution.py:490
  (14 shorter events, 0.0 us)
Async XLA Ops:
  0.0 1.7 %copy-start = (f32[64,2,2,2304]{3,2,1,0:T(2,128)S(1)}, f32[64,2,2,2304]{3,2,1,0:T(2,128)}, u32[]{:S(2)}) copy-start(f32[64,2,2,2304]{3,2,1,0:T(2,128)} %param.21) | copy-start | bytes 7077892
  2.0 4.2 %copy-start.8 = (bf16[576,4096]{1,0:T(8,128)(2,1)S(1)}, bf16[576,4096]{1,0:T(8,128)(2,1)}, u32[]{:S(2)}) copy-start(bf16[576,4096]{1,0:T(8,128)(2,1)} %param.16) | copy-start | bytes 14155780
  2.0 4.4 %copy-start.9 = (bf16[128,4096]{1,0:T(8,128)(2,1)S(1)}, bf16[128,4096]{1,0:T(8,128)(2,1)}, u32[]{:S(2)}) copy-start(bf16[128,4096]{1,0:T(8,128)(2,1)} %param.14) | copy-start | bytes 3145732
  2.0 5.9 %slice-start.2 = ((s8[4718592]{0:T(1024)(128)(4,1)}), s8[4194304]{0:T(1024)(128)(4,1)S(1)}, s32[]{:S(2)}) async-start(s8[4718592]{0:T(1024)(128)(4,1)} %bitcast.20), calls=%async_computation.2 | async-start | bytes 8388608
  6.2 1.7 %slice-start.3 = ((s8[4718592]{0:T(1024)(128)(4,1)}), s8[524288]{0:T(1024)(128)(4,1)S(1)}, s32[]{:S(2)}) async-start(s8[4718592]{0:T(1024)(128)(4,1)} %bitcast.20), calls=%async_computation.3 | async-start | bytes 1048576
  6.4 32.8 %slice-start = ((s8[4718592]{0:T(1024)(128)(4,1)}), s8[4194304]{0:T(1024)(128)(4,1)S(1)}, s32[]{:S(2)}) async-start(s8[4718592]{0:T(1024)(128)(4,1)} %bitcast.18), calls=%async_computation | async-start | bytes 8388608
  7.8 1.5 %copy-start.1 = (f32[2,32,1024]{2,1,0:T(8,128)S(1)}, f32[2,32,1024]{2,1,0:T(8,128)}, u32[]{:S(2)}) copy-start(f32[2,32,1024]{2,1,0:T(8,128)} %constant.25.clone.fine_ref) | copy-start | bytes 786436
  7.8 1.5 %copy-start.2 = (f32[2,32,1024]{2,1,0:T(8,128)S(1)}, f32[2,32,1024]{2,1,0:T(8,128)}, u32[]{:S(2)}) copy-start(f32[2,32,1024]{2,1,0:T(8,128)} %constant.24.clone.coarse_ref) | copy-start | bytes 786436
  7.9 1.5 %copy-start.3 = (f32[33,1024]{1,0:T(8,128)S(1)}, f32[33,1024]{1,0:T(8,128)}, u32[]{:S(2)}) copy-start(f32[33,1024]{1,0:T(8,128)} %constant.23.clone.feats_ref) | copy-start | bytes 405508
  7.9 1.5 %copy-start.4 = (f32[64,64]{1,0:T(8,128)S(1)}, f32[64,64]{1,0:T(8,128)}, u32[]{:S(2)}) copy-start(f32[64,64]{1,0:T(8,128)} %mid_ref.1) | copy-start | bytes 49156
  7.9 1.5 %copy-start.5 = (f32[3,3,576]{2,1,0:T(4,128)S(1)}, f32[3,3,576]{2,1,0:T(4,128)}, u32[]{:S(2)}) copy-start(f32[3,3,576]{2,1,0:T(4,128)} %short_ref.1) | copy-start | bytes 62212
  7.9 1.5 %copy-start.6 = (f32[33,64]{1,0:T(8,128)S(1)}, f32[33,64]{1,0:T(8,128)}, u32[]{:S(2)}) copy-start(f32[33,64]{1,0:T(8,128)} %in_ref.1) | copy-start | bytes 25348
  7.9 1.5 %copy-start.7 = (f32[2,576]{1,0:T(2,128)S(1)}, f32[2,576]{1,0:T(2,128)}, u32[]{:S(2)}) copy-start(f32[2,576]{1,0:T(2,128)} %skip_ref.1) | copy-start | bytes 13828
  8.0 31.3 %slice-start.1 = ((s8[4718592]{0:T(1024)(128)(4,1)}), s8[524288]{0:T(1024)(128)(4,1)S(1)}, s32[]{:S(2)}) async-start(s8[4718592]{0:T(1024)(128)(4,1)} %bitcast.18), calls=%async_computation.1 | async-start | bytes 1048576

commit v2 on v1

--- a/solution.py
+++ b/solution.py
@@ -249,15 +249,39 @@
     return jnp.sum(jnp.where(lanes == wanted, vector, 0.0), axis=1, keepdims=True)
 
 
-def kernel_spectra(chan_dev, in_ref, mid_ref, out_ref, rate_ref, feats_ref, cos_ref, sin_ref):
+def window_tile(chan_dev, total_width):
+    start = (lax.axis_index("col") * lax.axis_size("row") + lax.axis_index("row")) * chan_dev
+    tile = start // 128
+    return tile - tile // (total_width // 128 - 1), start
+
+
+def window_picks(chan_dev, total_width, window):
+    tile, start = window_tile(chan_dev, total_width)
+    lanes = lax.broadcasted_iota(jnp.int32, (chan_dev, window), 1)
+    wanted = lax.broadcasted_iota(jnp.int32, (chan_dev, window), 0) + (start - tile * 128)
+    return jnp.where(lanes == wanted, 1.0, 0.0)
+
+
+def kernel_spectra(chan_dev, total_width, in_ref, mid_ref, out_ref, rate_ref, feats_ref, cos_ref, sin_ref):
     hidden = jnp.sin(exact_dot(in_ref[...], feats_ref[...], 0))
     hidden = jnp.sin(exact_dot(mid_ref[...], hidden, 0))
     decay = jnp.exp(-feats_ref[0:1, :] * own_column(rate_ref[...], chan_dev))
     not_first = lax.broadcasted_iota(jnp.int32, decay.shape, 1) > 0
     sums, differences = [], []
+    picks = window_picks(chan_dev, total_width, out_ref.shape[3])
     for order in range(2):
-        ahead = exact_dot(out_ref[order, 0], hidden, 1) * decay
-        behind = jnp.where(not_first, exact_dot(out_ref[order, 1], hidden, 1) * decay, 0.0)
+        own = [
+            lax.dot_general(
+                picks,
+                out_ref[:, order, direction, :],
+                (((1,), (1,)), ((), ())),
+                precision=HIGHEST,
+                preferred_element_type=jnp.float32,
+            )
+            for direction in range(2)
+        ]
+        ahead = exact_dot(own[0], hidden, 1) * decay
+        behind = jnp.where(not_first, exact_dot(own[1], hidden, 1) * decay, 0.0)
         sums.append(ahead + behind)
         differences.append(ahead - behind)
     scale = 1.0 / cos_ref.shape[0]
@@ -296,23 +320,17 @@
     n_rows,
     n_cols,
     chan_dev,
-    value_ref,
-    first_ref,
-    second_ref,
-    short_ref,
-    in_ref,
-    mid_ref,
-    out_ref,
-    rate_ref,
-    skip_ref,
-    feats_ref,
-    coarse_ref,
-    fine_ref,
-    gathered_ref,
+    total_width,
+    sources,
+    result_ref,
+    held,
     cos_ref,
     sin_ref,
+    projected_ref,
     moved_ref,
     y_ref,
+    gathered,
+    load_sem,
     there_send,
     there_recv,
     back_send,
@@ -327,7 +345,16 @@
     block_len = moved_ref.shape[3]
     half = n_cols // 2
     mate = col + 1 - 2 * (col % 2)
-    projected = (value_ref, first_ref, second_ref)
+    gathered_ref = result_ref if gathered is None else gathered
+    tile, _ = window_tile(chan_dev, total_width)
+    lanes = pl.ds(pl.multiple_of(tile * 128, 128), held["filter_out"].shape[3])
+    loads = {}
+    for index, name in enumerate(sources):
+        source = sources[name]
+        if name == "filter_out":
+            source = source.at[:, :, :, lanes]
+        loads[name] = pltpu.make_async_copy(source, held[name], load_sem.at[index])
+        loads[name].start()
 
     def copy(source, target, send_sem, recv_sem, to_row, to_col):
         return pltpu.make_async_remote_copy(
@@ -350,13 +377,33 @@
     barrier = pltpu.get_barrier_semaphore()
     for partner in partners:
         pl.semaphore_signal(barrier, inc=1, device_id=partner, device_id_type=pl.DeviceIdType.MESH)
-    pl.semaphore_wait(barrier, len(partners))
+    for name in ("coarse", "fine"):
+        loads[name].wait()
+    make_tables(held["coarse"], held["fine"], cos_ref, sin_ref)
+    loads["tokens"].wait()
 
     there = {}
-    for which in range(3):
+    for which, name in enumerate(("w_value", "w_first", "w_second")):
+        loads[name].wait()
+        rows = held[name].shape[0] // 2
+        for part in range(2):
+            product = lax.dot_general(
+                held[name][part * rows : (part + 1) * rows, :],
+                held["tokens"][...],
+                (((1,), (1,)), ((), ())),
+                preferred_element_type=jnp.float32,
+            )
+            blocks = n_rows // 2
+            for s in range(blocks):
+                projected_ref[which, part * blocks + s] = product[
+                    s * chan_dev : (s + 1) * chan_dev
+                ].astype(jnp.bfloat16)
+        moved_ref[which, row] = projected_ref[which, row]
+        if which == 0:
+            pl.semaphore_wait(barrier, len(partners))
         for d in range(1, n_rows):
             there[which, d] = copy(
-                projected[which].at[row_at(d)],
+                projected_ref.at[which, row_at(d)],
                 moved_ref.at[which, row],
                 there_send.at[which, d - 1],
                 there_recv.at[which, d - 1],
@@ -364,20 +411,29 @@
                 col,
             )
             there[which, d].start()
-    for which in range(3):
-        moved_ref[which, row] = projected[which][row]
-
-    make_tables(coarse_ref, fine_ref, cos_ref, sin_ref)
-    spectra = kernel_spectra(chan_dev, in_ref, mid_ref, out_ref, rate_ref, feats_ref, cos_ref, sin_ref)
+
+    for name in ("filter_in", "filter_mid", "filter_out", "rate", "feats", "short_taps", "skip"):
+        loads[name].wait()
+    spectra = kernel_spectra(
+        chan_dev,
+        total_width,
+        held["filter_in"],
+        held["filter_mid"],
+        held["filter_out"],
+        held["rate"],
+        held["feats"],
+        cos_ref,
+        sin_ref,
+    )
 
     def signal_of(which):
         for d in range(1, n_rows):
             there[which, d].wait_recv()
         return short_rows(
-            [moved_ref[which, s] for s in range(n_rows)], short_ref, which, chan_dev
+            [moved_ref[which, s] for s in range(n_rows)], held["short_taps"], which, chan_dev
         )
 
-    signal = long_convolutions(signal_of, spectra, skip_ref, cos_ref, sin_ref, chan_dev)
+    signal = long_convolutions(signal_of, spectra, held["skip"], cos_ref, sin_ref, chan_dev)
     for s in range(n_rows):
         y_ref[s] = signal[:, s * block_len : (s + 1) * block_len].astype(jnp.bfloat16)
     gathered_ref[col, row] = y_ref[row]
@@ -410,15 +466,37 @@
             )
             far[h, d].start()
         to_mate(0, d)
+    group = n_rows * chan_dev
+
+    def add_group(owner, total):
+        left = jnp.concatenate(
+            [gathered_ref[owner, s].astype(jnp.float32) for s in range(n_rows)], axis=0
+        ).astype(jnp.bfloat16)
+        rows = pl.ds(pl.multiple_of(owner * group, group), group)
+        product = lax.dot_general(
+            left,
+            held["w_out"][rows, :],
+            (((0,), (0,)), ((), ())),
+            preferred_element_type=jnp.float32,
+        )
+        return product if total is None else total + product
+
+    loads["w_out"].wait()
+    total = add_group(col, None)
     for h in range(1, half):
         for d in range(n_rows):
             far[h, d].wait_recv()
             to_mate(half - h, d)
+    for h in range(half):
+        if h:
+            total = add_group(far_at(h), total)
+        for d in range(n_rows):
+            near[h, d].wait_recv()
+        total = add_group((mate + 2 * h) % n_cols, total)
+    result_ref[...] = total.astype(jnp.bfloat16)
     for send in (there, back, far, near):
         for one in send.values():
             one.wait_send()
-    for one in near.values():
-        one.wait_recv()
 
 
 def on_device_dense(
@@ -435,34 +513,51 @@
     w_out,
 ):
     n_rows = lax.axis_size("row")
-    row_index = lax.axis_index("row")
-    col_index = lax.axis_index("col")
+    n_cols = lax.axis_size("col")
+    half = n_cols // 2
     local_width = w_value.shape[0]
     chan_dev = local_width // n_rows
+    total_width = filter_out.shape[3]
     block_len = tokens.shape[0]
     seq_len = n_rows * block_len
-    projected = [
-        jnp.einsum("td,cd->ct", tokens, weight, preferred_element_type=jnp.float32)
-        .astype(jnp.bfloat16)
-        .reshape(n_rows, chan_dev, block_len)
-        for weight in (w_value, w_gate_one, w_gate_two)
-    ]
-    global_start = col_index * local_width + row_index * chan_dev
-    own_out = lax.dynamic_slice_in_dim(filter_out, global_start, chan_dev, 3).transpose(1, 2, 3, 0)
     coarse, fine = table_seeds(seq_len)
-    n_cols = lax.axis_size("col")
-    half = n_cols // 2
+    sources = dict(
+        tokens=tokens,
+        coarse=coarse,
+        fine=fine,
+        w_value=w_value,
+        w_first=w_gate_one,
+        w_second=w_gate_two,
+        filter_out=filter_out,
+        filter_in=filter_in,
+        filter_mid=filter_mid,
+        rate=decay_rate.reshape(1, local_width),
+        feats=position_features(seq_len),
+        short_taps=short_taps,
+        skip=skip,
+        w_out=w_out,
+    )
+    window = -(-(chan_dev + 127) // 128) * 128
+    held = {name: pltpu.VMEM(source.shape, source.dtype) for name, source in sources.items()}
+    held["filter_out"] = pltpu.VMEM(filter_out.shape[:3] + (window,), filter_out.dtype)
     dma = pltpu.SemaphoreType.DMA
-    gathered = pl.pallas_call(
-        functools.partial(mix_kernel, n_rows, n_cols, chan_dev),
-        out_shape=jax.ShapeDtypeStruct((n_cols, n_rows, chan_dev, block_len), jnp.bfloat16),
-        in_specs=[pl.BlockSpec(memory_space=pltpu.VMEM)] * 12,
+    collected = (n_cols, n_rows, chan_dev, block_len)
+    result = jax.ShapeDtypeStruct((block_len, w_out.shape[1]), jnp.bfloat16)
+    gathered = pltpu.VMEM(collected, jnp.bfloat16)
+    return_value = pl.pallas_call(
+        functools.partial(mix_kernel, n_rows, n_cols, chan_dev, total_width),
+        out_shape=result,
+        in_specs=[{name: pl.BlockSpec(memory_space=pl.ANY) for name in sources}],
         out_specs=pl.BlockSpec(memory_space=pltpu.VMEM),
         scratch_shapes=[
+            held,
             pltpu.VMEM((seq_len, seq_len), jnp.bfloat16),
             pltpu.VMEM((seq_len, seq_len), jnp.bfloat16),
             pltpu.VMEM((3, n_rows, chan_dev, block_len), jnp.bfloat16),
+            pltpu.VMEM((3, n_rows, chan_dev, block_len), jnp.bfloat16),
             pltpu.VMEM((n_rows, chan_dev, block_len), jnp.bfloat16),
+            gathered,
+            dma((len(sources),)),
             dma((3, n_rows - 1)),
             dma((3, n_rows - 1)),
             dma((n_rows - 1,)),
@@ -473,27 +568,10 @@
             dma((half, n_rows)),
         ],
         compiler_params=pltpu.CompilerParams(
-            vmem_limit_bytes=26 << 20, collective_id=0, has_side_effects=True
+            vmem_limit_bytes=56 << 20, collective_id=0, has_side_effects=True
         ),
-    )(
-        *projected,
-        short_taps,
-        filter_in,
-        filter_mid,
-        own_out,
-        decay_rate.reshape(1, local_width),
-        skip,
-        position_features(seq_len),
-        coarse,
-        fine,
-    )
-    totals = jnp.einsum(
-        "ct,cd->td",
-        gathered.reshape(n_cols * local_width, block_len),
-        w_out,
-        preferred_element_type=jnp.float32,
-    )
-    return totals.astype(jnp.bfloat16)
+    )(sources)
+    return return_value
 
 
 def solution(mesh):
@@ -521,6 +599,10 @@
             and w_value.shape[0] // devices % 8 == 0
             and columns % 2 == 0
             and columns > 2
+            and mesh.shape["row"] % 2 == 0
+            and rest[5].shape[3] % 128 == 0
+            and w_value.shape[0] // devices <= 129
+            and rest[5].shape[3] >= 384
         )
         body = on_device_dense if dense else on_device
         return jax.shard_map(

time: 40.9 us -> 40.1 us (0.980)
  matrix products: 8.56 us -> 0 us
  Pallas kernels: 29.8 us -> 36.9 us
  local copies, waits for them, and re-layouts: 2.19 us -> 2.94 us
    dot_general x4 -> x0, matrix products: 8.56 us -> none  [the longest x3 7.03 us: on_device_dense(): jnp.einsum('td,cd->ct', tokens, weight, preferred_element_type=jnp.float32)]
    pallas_call x1, Pallas kernels: 29.8 us -> 36.9 us  [on_device_dense(): pl.pallas_call(functools.partial(mix_kernel, n_rows, n_cols, chan_dev, to...]
    unnamed x29 -> x1, local copies, waits for them, and re-layouts: 1.15 us -> 1.67 us
    reshape x1, local copies, waits for them, and re-layouts: 0.84 us -> 1.27 us  [on_device_dense(): decay_rate.reshape(1, local_width)]
where the time goes in v2:
time: 40.1 us; the launch traced here: 39.9 us
  Pallas kernels  36.9 us (92%)
  local copies, waits for them, and re-layouts  2.94 us (7%)
    pallas_call x1, Pallas kernels, on_device_dense(): pl.pallas_call(functools.partial(mix_kernel, n_rows, n_cols, chan_dev, to...  36.9 us
    unnamed x1, local copies, waits for them, and re-layouts  1.67 us
    reshape x1, local copies, waits for them, and re-layouts, on_device_dense(): decay_rate.reshape(1, local_width)  1.27 us

profile of v2, /device:TPU:0, one launch (start us, length us, event | category | flops | bytes accessed | tf_op | source)
XLA Modules:
  0.0 39.9 jit_solution(18306904489243644308)
XLA Ops:
  0.0 1.3 %reshape.3.sources__rate__ = f32[1,576]{1,0:T(1,128)} reshape(f32[576]{0:T(1024)} %param.22) | data formatting | bytes 4608 | tf_op jit(solution)/shard_map/reshape | solution.py:534
  1.3 36.9 %shard_map.136 = bf16[128,1024]{1,0:T(8,128)(2,1)} custom-call(f32[2,32,1024]{2,1,0:T(8,128)} %constant.6.clone.sources__coarse__, f32[33,1024]{1,0:T(8,128)} %constant.7.clone.sources__feats__, f32[33,64]{1,0:T(8,128)} %sources__filter_in__.1, f32[64,64]{1,0:T(8,128)} %sources__filter_mid__.1, f32[64,2,2,2304]{3,2,1,0:T(2,128)} %sources__filter_out__.1, ...), custom_call_target="tpu_custom_call" | custom-call | tf_op jit(solution)/shard_map/pallas_call | solution.py:547
  38.2 1.7 %copy.16 = bf16[128,1024]{1,0:T(8,128)(2,1)} copy(bf16[128,1024]{1,0:T(8,128)(2,1)} %shard_map.136) | data formatting | bytes 524288

commit v3 on v2

--- a/solution.py
+++ b/solution.py
@@ -316,6 +316,13 @@
     return signal
 
 
+def flipped(index, mask):
+    for bit in range(mask.bit_length()):
+        if mask >> bit & 1:
+            index = index + (1 - 2 * (index // 2**bit % 2)) * 2**bit
+    return index
+
+
 def mix_kernel(
     n_rows,
     n_cols,
@@ -331,6 +338,7 @@
     y_ref,
     gathered,
     load_sem,
+    weight_sem,
     there_send,
     there_recv,
     back_send,
@@ -349,12 +357,32 @@
     tile, _ = window_tile(chan_dev, total_width)
     lanes = pl.ds(pl.multiple_of(tile * 128, 128), held["filter_out"].shape[3])
     loads = {}
-    for index, name in enumerate(sources):
-        source = sources[name]
-        if name == "filter_out":
-            source = source.at[:, :, :, lanes]
-        loads[name] = pltpu.make_async_copy(source, held[name], load_sem.at[index])
-        loads[name].start()
+    pairs = list(range(1, n_rows // 2))[::-1]
+    pairs = [p for p in pairs if p >= n_rows // 4] + [p for p in pairs if p < n_rows // 4] + [0]
+    pair_rows = 2 * chan_dev
+
+    def load(*names):
+        for name in names:
+            source = sources[name]
+            if name == "filter_out":
+                source = source.at[:, :, :, lanes]
+            index = list(sources).index(name)
+            loads[name] = pltpu.make_async_copy(source, held[name], load_sem.at[index])
+            loads[name].start()
+
+    def weight_rows(pair):
+        return pl.ds(pl.multiple_of(flipped(row // 2, pair) * pair_rows, pair_rows), pair_rows)
+
+    def load_weight(which, name):
+        for pair in pairs:
+            rows = weight_rows(pair)
+            loads[which, pair] = pltpu.make_async_copy(
+                sources[name].at[rows, :], held[name].at[rows, :], weight_sem.at[which, pair]
+            )
+            loads[which, pair].start()
+
+    load("coarse", "fine", "tokens")
+    load_weight(0, "w_value")
 
     def copy(source, target, send_sem, recv_sem, to_row, to_col):
         return pltpu.make_async_remote_copy(
@@ -366,8 +394,8 @@
             device_id_type=pl.DeviceIdType.MESH,
         )
 
-    def row_at(offset):
-        return (row + offset) % n_rows
+    def row_at(mask):
+        return flipped(row, mask)
 
     def far_at(offset):
         return (col + 2 * offset) % n_cols
@@ -380,37 +408,44 @@
     for name in ("coarse", "fine"):
         loads[name].wait()
     make_tables(held["coarse"], held["fine"], cos_ref, sin_ref)
+    load_weight(1, "w_first")
+    load("filter_in", "filter_mid", "filter_out", "rate", "feats", "short_taps", "skip")
     loads["tokens"].wait()
 
     there = {}
     for which, name in enumerate(("w_value", "w_first", "w_second")):
-        loads[name].wait()
-        rows = held[name].shape[0] // 2
-        for part in range(2):
+        for pair in pairs:
+            loads[which, pair].wait()
             product = lax.dot_general(
-                held[name][part * rows : (part + 1) * rows, :],
+                held[name][weight_rows(pair), :],
                 held["tokens"][...],
                 (((1,), (1,)), ((), ())),
                 preferred_element_type=jnp.float32,
             )
-            blocks = n_rows // 2
-            for s in range(blocks):
-                projected_ref[which, part * blocks + s] = product[
-                    s * chan_dev : (s + 1) * chan_dev
-                ].astype(jnp.bfloat16)
-        moved_ref[which, row] = projected_ref[which, row]
+            for s in range(2):
+                target = flipped(row // 2, pair) * 2 + s
+                projected_ref[which, target] = product[s * chan_dev : (s + 1) * chan_dev].astype(
+                    jnp.bfloat16
+                )
+            if which == 0 and pair == pairs[0]:
+                pl.semaphore_wait(barrier, len(partners))
+            for d in (2 * pair, 2 * pair + 1):
+                if d == 0:
+                    moved_ref[which, row] = projected_ref[which, row]
+                    continue
+                there[which, d] = copy(
+                    projected_ref.at[which, row_at(d)],
+                    moved_ref.at[which, row],
+                    there_send.at[which, d - 1],
+                    there_recv.at[which, d - 1],
+                    row_at(d),
+                    col,
+                )
+                there[which, d].start()
         if which == 0:
-            pl.semaphore_wait(barrier, len(partners))
-        for d in range(1, n_rows):
-            there[which, d] = copy(
-                projected_ref.at[which, row_at(d)],
-                moved_ref.at[which, row],
-                there_send.at[which, d - 1],
-                there_recv.at[which, d - 1],
-                row_at(d),
-                col,
-            )
-            there[which, d].start()
+            load_weight(2, "w_second")
+        if which == 1:
+            load("w_out")
 
     for name in ("filter_in", "filter_mid", "filter_out", "rate", "feats", "short_taps", "skip"):
         loads[name].wait()
@@ -439,7 +474,8 @@
     gathered_ref[col, row] = y_ref[row]
 
     back = {}
-    for d in range(1, n_rows):
+    far_first = [2 * pair + x for pair in pairs for x in range(2) if pair or x]
+    for d in far_first:
         back[d] = copy(
             y_ref.at[row_at(d)],
             gathered_ref.at[col, row],
@@ -452,14 +488,15 @@
     far, near = {}, {}
 
     def to_mate(h, d):
-        block = gathered_ref.at[far_at(h), row_at(n_rows - d)]
+        block = gathered_ref.at[far_at(h), row_at(d)]
         near[h, d] = copy(block, block, mate_send.at[h, d], mate_recv.at[h, d], row, mate)
         near[h, d].start()
 
-    for d in range(n_rows):
+    near_first = [0] + far_first[::-1]
+    for d in near_first:
         if d:
             back[d].wait_recv()
-        block = gathered_ref.at[col, row_at(n_rows - d)]
+        block = gathered_ref.at[col, row_at(d)]
         for h in range(1, half):
             far[h, d] = copy(
                 block, block, far_send.at[h - 1, d], far_recv.at[h - 1, d], row, far_at(h)
@@ -484,7 +521,7 @@
     loads["w_out"].wait()
     total = add_group(col, None)
     for h in range(1, half):
-        for d in range(n_rows):
+        for d in near_first:
             far[h, d].wait_recv()
             to_mate(half - h, d)
     for h in range(half):
@@ -558,6 +595,7 @@
             pltpu.VMEM((n_rows, chan_dev, block_len), jnp.bfloat16),
             gathered,
             dma((len(sources),)),
+            dma((3, n_rows // 2)),
             dma((3, n_rows - 1)),
             dma((3, n_rows - 1)),
             dma((n_rows - 1,)),
@@ -599,7 +637,8 @@
             and w_value.shape[0] // devices % 8 == 0
             and columns % 2 == 0
             and columns > 2
-            and mesh.shape["row"] % 2 == 0
+            and mesh.shape["row"] >= 4
+            and mesh.shape["row"] & (mesh.shape["row"] - 1) == 0
             and rest[5].shape[3] % 128 == 0
             and w_value.shape[0] // devices <= 129
             and rest[5].shape[3] >= 384

time: 40.1 us -> 41 us (1.022)
  Pallas kernels: 36.9 us -> 37.9 us
    pallas_call x1, Pallas kernels: 36.9 us -> 37.9 us  [on_device_dense(): pl.pallas_call(functools.partial(mix_kernel, n_rows, n_cols, chan_dev, to...]
where the time goes in v3:
time: 41 us; the launch traced here: 40.8 us
  Pallas kernels  37.9 us (92%)
  local copies, waits for them, and re-layouts  2.94 us (7%)
    pallas_call x1, Pallas kernels, on_device_dense(): pl.pallas_call(functools.partial(mix_kernel, n_rows, n_cols, chan_dev, to...  37.9 us
    unnamed x1, local copies, waits for them, and re-layouts  1.67 us
    reshape x1, local copies, waits for them, and re-layouts, on_device_dense(): decay_rate.reshape(1, local_width)  1.27 us

profile of v3, /device:TPU:0, one launch (start us, length us, event | category | flops | bytes accessed | tf_op | source)
XLA Modules:
  0.0 40.8 jit_solution(9093040117875737572)
XLA Ops:
  0.0 1.3 %reshape.3.sources__rate__ = f32[1,576]{1,0:T(1,128)} reshape(f32[576]{0:T(1024)} %param.22) | data formatting | bytes 4608 | tf_op jit(solution)/shard_map/reshape | solution.py:571
  1.3 37.9 %shard_map.136 = bf16[128,1024]{1,0:T(8,128)(2,1)} custom-call(f32[2,32,1024]{2,1,0:T(8,128)} %constant.6.clone.sources__coarse__, f32[33,1024]{1,0:T(8,128)} %constant.7.clone.sources__feats__, f32[33,64]{1,0:T(8,128)} %sources__filter_in__.1, f32[64,64]{1,0:T(8,128)} %sources__filter_mid__.1, f32[64,2,2,2304]{3,2,1,0:T(2,128)} %sources__filter_out__.1, ...), custom_call_target="tpu_custom_call" | custom-call | tf_op jit(solution)/shard_map/pallas_call | solution.py:584
  39.1 1.7 %copy.16 = bf16[128,1024]{1,0:T(8,128)(2,1)} copy(bf16[128,1024]{1,0:T(8,128)(2,1)} %shard_map.136) | data formatting | bytes 524288
